TPU v7x, 32 devices: a whole 2x2x4 slice. The times are simulated.
32 devices in a mesh: sp: 4 (over z), fs: 4 (over y, x), tp: 2 (over core).
Axes of the slice: x: 2, y: 2, z: 4, core: 2. Of those that a mesh axis runs over, the one named last changes fastest.
Arguments:
- tokens: bfloat16 [2048, 2048], P('sp', ('fs', 'tp')), may hold values from -6 to 6
- in_gain: float32 [2048], replicated, may hold values from 0.1 to 1.9
- conv_a_weight: bfloat16 [2048, 1024], P(None, ('fs', 'tp')), may hold values from -0.125 to 0.125
- conv_gate_weight: bfloat16 [2048, 1024], P(None, ('fs', 'tp')), may hold values from -0.125 to 0.125
- query_weight: bfloat16 [2048, 1024], P(None, ('fs', 'tp')), may hold values from -0.125 to 0.125
- key_weight: bfloat16 [2048, 1024], P(None, ('fs', 'tp')), may hold values from -0.125 to 0.125
- value_weight: bfloat16 [2048, 1024], P(None, ('fs', 'tp')), may hold values from -0.125 to 0.125
- conv_taps: bfloat16 [31, 1024], replicated, may hold values from -3 to 3
- conv_norm_gain: float32 [1024], replicated, may hold values from 0.1 to 1.9
- break_shift: bfloat16 [16, 2048], P(('fs', 'tp'), 'sp'), may hold values from -20 to 1
- conv_out_gain: float32 [1024], replicated, may hold values from 0.1 to 1.9
- attn_out_gain: float32 [1024], replicated, may hold values from 0.1 to 1.9
- out_weight: bfloat16 [2048, 2048], P(None, ('fs', 'tp')), may hold values from -0.125 to 0.125
Outputs:
- mixed: bfloat16 [2048, 2048], P('sp', ('fs', 'tp'))
All inputs are finite; a program needn't handle non-finite values.
Results may differ from a plain program's by a relative error of at most 0.0078.
Values may be sent and summed in bfloat16 or wider, within the bound.
A program may use at most 128 MiB of HBM per device.

v0:
```python
import jax
import jax.numpy as jnp
from jax import lax
from jax.sharding import PartitionSpec as P

HEAD_DIM = 64


epsilon = 1e-06


def passed_along(shard, axis, by):
    count = lax.axis_size(axis)
    pairs = [(i, i + by) for i in range(count) if 0 <= i + by < count]
    return lax.ppermute(shard, axis, pairs)


def per_device(
    tokens,
    in_gain,
    conv_a_weight,
    conv_gate_weight,
    query_weight,
    key_weight,
    value_weight,
    conv_taps,
    conv_norm_gain,
    break_shift,
    conv_out_gain,
    attn_out_gain,
    out_weight,
):
    rows_here = tokens.shape[0]
    model_width = in_gain.shape[0]
    channels = model_width // 2
    local_width = conv_a_weight.shape[1]
    heads_here = break_shift.shape[0]
    group_index = lax.axis_index(("fs", "tp"))
    shard_index = lax.axis_index("sp")
    stacked = jnp.concatenate(
        (conv_a_weight, conv_gate_weight, query_weight, key_weight, value_weight), axis=1
    )
    segment = lax.all_gather(tokens, ("fs", "tp"), axis=1, tiled=True)
    segment_wide = segment.astype(jnp.float32)
    scaled = (segment_wide * in_gain[None, :]).astype(jnp.bfloat16)
    totals = jnp.dot(scaled, stacked, preferred_element_type=jnp.float32)
    totals, squares = (totals, jnp.sum(segment_wide * segment_wide, axis=1))
    input_scale = lax.rsqrt(squares / model_width + epsilon)
    projected = (totals * input_scale[:, None]).astype(jnp.bfloat16)
    conv_a = projected[:, :local_width]
    conv_gate = projected[:, local_width : 2 * local_width]
    query = projected[:, 2 * local_width : 3 * local_width]
    key = projected[:, 3 * local_width : 4 * local_width]
    value = projected[:, 4 * local_width :]
    gated_input = conv_a.astype(jnp.float32) * jax.nn.sigmoid(conv_gate.astype(jnp.float32))
    reach_rows = conv_taps.shape[0] - 1
    earlier = passed_along(gated_input[rows_here - reach_rows :], "sp", 1)
    padded = jnp.concatenate((earlier, gated_input), axis=0)
    tap_values = lax.dynamic_slice_in_dim(
        conv_taps, group_index * local_width, local_width, 1
    ).astype(jnp.float32)
    conv_out = jnp.zeros((rows_here, local_width), jnp.float32)
    for offset in range(reach_rows + 1):
        conv_out = conv_out + tap_values[offset][None, :] * padded[offset : offset + rows_here]
    first_sum, second_sum = lax.psum(
        (jnp.sum(conv_out, axis=1), jnp.sum(conv_out * conv_out, axis=1)), ("fs", "tp")
    )
    row_mean = first_sum / channels
    row_spread = second_sum / channels - row_mean * row_mean
    centered = conv_out - row_mean[:, None]
    norm_gain = lax.dynamic_slice_in_dim(conv_norm_gain, group_index * local_width, local_width, 0)
    normed = centered * lax.rsqrt(row_spread + epsilon)[:, None] * norm_gain[None, :]
    conv_mixed = jax.nn.silu(normed).astype(jnp.bfloat16)
    queries = query.reshape(rows_here, heads_here, HEAD_DIM)
    query_pos = shard_index * rows_here + jnp.arange(rows_here, dtype=jnp.int32)
    score_scale = HEAD_DIM ** (-0.5)

    def attend(running, key_rows, value_rows, shift_rows, start_pos):
        outputs, behind = running
        piece_rows = key_rows.shape[0]
        key_heads = key_rows.reshape(piece_rows, heads_here, HEAD_DIM)
        value_heads = value_rows.reshape(piece_rows, heads_here, HEAD_DIM)
        scores = (
            jnp.einsum("qhd,khd->hqk", queries, key_heads, preferred_element_type=jnp.float32)
            * score_scale
        )
        scores = scores + shift_rows.astype(jnp.float32)[:, None, :]
        key_pos = start_pos + jnp.arange(piece_rows, dtype=jnp.int32)
        allowed = ((key_pos[None, :] < query_pos[:, None]) & (key_pos[None, :] >= 0))[None]
        log_fail = jnp.where(allowed, jax.nn.log_sigmoid(-scores), 0.0)
        later_sum = lax.cumsum(log_fail, axis=2, reverse=True) - log_fail + behind[:, :, None]
        weights = jnp.where(allowed, jnp.exp(jax.nn.log_sigmoid(scores) + later_sum), 0.0).astype(
            jnp.bfloat16
        )
        outputs = outputs + jnp.einsum(
            "hqk,khd->qhd", weights, value_heads, preferred_element_type=jnp.float32
        )
        return (outputs, behind + jnp.sum(log_fail, axis=2))

    start_state = (
        jnp.zeros((rows_here, heads_here, HEAD_DIM), jnp.float32),
        jnp.zeros((heads_here, rows_here), jnp.float32),
    )
    all_keys, all_values, all_shifts = (
        lax.all_gather(key, "sp", axis=0, tiled=True),
        lax.all_gather(value, "sp", axis=0, tiled=True),
        lax.all_gather(break_shift, "sp", axis=1, tiled=True),
    )
    sp_count = lax.axis_size("sp")
    grouped = 1
    while grouped * 2 * rows_here <= 1024 and sp_count % (grouped * 2) == 0:
        grouped = grouped * 2
    block_rows = grouped * rows_here
    last_block = (shard_index * rows_here + rows_here - 1) // block_rows

    def advance(counter, running):
        begin_row = (last_block - counter) * block_rows
        key_rows = lax.dynamic_slice_in_dim(all_keys, begin_row, block_rows, 0)
        value_rows = lax.dynamic_slice_in_dim(all_values, begin_row, block_rows, 0)
        shift_rows = lax.dynamic_slice_in_dim(all_shifts, begin_row, block_rows, 1)
        return attend(running, key_rows, value_rows, shift_rows, begin_row)

    outputs, behind = lax.fori_loop(0, last_block + 1, advance, start_state)
    attn_mixed = outputs.reshape(rows_here, heads_here * HEAD_DIM).astype(jnp.bfloat16)
    conv_piece = lax.all_gather(conv_mixed, ("fs", "tp"), axis=1, tiled=True)
    attn_piece = lax.all_gather(attn_mixed, ("fs", "tp"), axis=1, tiled=True)
    piece_width = conv_piece.shape[1]
    conv_wide = conv_piece.astype(jnp.float32)
    attn_wide = attn_piece.astype(jnp.float32)
    conv_scaled = (conv_wide * conv_out_gain[None, :]).astype(jnp.bfloat16)
    attn_scaled = (attn_wide * attn_out_gain[None, :]).astype(jnp.bfloat16)
    conv_rows = lax.slice_in_dim(out_weight, 0, piece_width, axis=0)
    attn_rows = lax.dynamic_slice_in_dim(out_weight, channels, piece_width, 0)
    conv_total = jnp.dot(conv_scaled, conv_rows, preferred_element_type=jnp.float32)
    attn_total = jnp.dot(attn_scaled, attn_rows, preferred_element_type=jnp.float32)
    conv_squares = jnp.sum(conv_wide * conv_wide, axis=1)
    attn_squares = jnp.sum(attn_wide * attn_wide, axis=1)
    conv_total, attn_total, conv_squares, attn_squares = (
        conv_total,
        attn_total,
        conv_squares,
        attn_squares,
    )
    conv_scale = lax.rsqrt(conv_squares / channels + epsilon)
    attn_scale = lax.rsqrt(attn_squares / channels + epsilon)
    mixed = conv_total * conv_scale[:, None] + attn_total * attn_scale[:, None]
    return mixed.astype(jnp.bfloat16)


def solution(mesh):
    return jax.shard_map(
        per_device,
        mesh=mesh,
        in_specs=(
            P("sp", ("fs", "tp")),
            P(),
            P(None, ("fs", "tp")),
            P(None, ("fs", "tp")),
            P(None, ("fs", "tp")),
            P(None, ("fs", "tp")),
            P(None, ("fs", "tp")),
            P(),
            P(),
            P(("fs", "tp"), "sp"),
            P(),
            P(),
            P(None, ("fs", "tp")),
        ),
        out_specs=P("sp", ("fs", "tp")),
        check_vma=False,
    )
```

profile of v0, /device:TPU:25, one launch (start us, length us, event | category | flops | bytes accessed | tf_op | source)
XLA Modules:
  0.0 199.4 jit_solution(11392080675907995282)
XLA Ops:
  7.3 8.5 %all_gather.22 = bf16[2,2048]{1,0:T(2,128)(2,1)S(1)} all-gather(bf16[2,512]{1,0:T(2,128)(2,1)} %param.24), channel_id=1, replica_groups=mesh['sp'=4,'fs'=4,'tp'=2] {'sp'}, dimensions={1}, use_global_device_ids=true | all-gather | bytes 10240 | tf_op jit(solution)/shard_map/all_gather | solution.py:107
  15.8 1.9 constant_dynamic-update-slice_fusion.4
  17.7 2.0 constant_dynamic-update-slice_fusion.3
  19.7 1.9 constant_dynamic-update-slice_fusion.2
  21.6 1.9 constant_dynamic-update-slice_fusion.1
  24.4 14.4 %all-gather.4.cloned.1.call-done = bf16[512,2048]{1,0:T(8,128)(2,1)} async-done(((bf16[512,256]{1,0:T(8,128)(2,1)}), bf16[512,2048]{1,0:T(8,128)(2,1)}) %all-gather.4.cloned.1.call-update) | async-done | bytes 2097168 | tf_op jit(solution)/shard_map/all_gather | solution.py:43
  38.7 2.1 %fusion.19 = f32[512]{0:T(512)S(1)} fusion(bf16[512,2048]{1,0:T(8,128)(2,1)} %all-gather.4.cloned.1.call-done), kind=kLoop, calls=%fused_computation.37 | loop fusion | flops 3145216 | bytes 2099200 | tf_op jit(solution)/shard_map/reduce_sum | solution.py:47
  40.8 4.2 %fusion.30 = bf16[512,640]{1,0:T(8,128)(2,1)S(1)} fusion(bf16[2048,640]{1,0:T(8,128)(2,1)} %constant_dynamic-update-slice_fusion, bf16[512,2048]{1,0:T(8,128)(2,1)} %all-gather.4.cloned.1.call-done, f32[2048]{0:T(1024)S(1)} %copy-done.4, f32[512]{0:T(512)S(1)} %add_rsqrt_fusion.3), kind=kOutput, calls=%fused_computation.78 | convolution fusion | flops 1345978368 | bytes 5384192 | tf_op jit(solution)/shard_map/dot_general | solution.py:46
  45.1 13.2 %all_gather.20 = bf16[2048,128]{1,0:T(8,128)(2,1)S(1)} all-gather(bf16[512,128]{1,0:T(8,128)(2,1)S(1)} %get-tuple-element.135), channel_id=1, replica_groups=mesh['sp'=4,'fs'=4,'tp'=2] {'sp'}, dimensions={0}, use_global_device_ids=true | all-gather | bytes 655360 | tf_op jit(solution)/shard_map/all_gather | solution.py:106
  58.3 13.7 %all_gather.21 = bf16[2048,128]{1,0:T(8,128)(2,1)S(1)} all-gather(bf16[512,128]{1,0:T(8,128)(2,1)S(1)} %get-tuple-element.134), channel_id=1, replica_groups=mesh['sp'=4,'fs'=4,'tp'=2] {'sp'}, dimensions={0}, use_global_device_ids=true | all-gather | bytes 655360 | tf_op jit(solution)/shard_map/all_gather | solution.py:105
  72.2 62.3 %while.13 = (s32[]{:T(128)}, f32[512,2,64]{0,2,1:T(8,128)S(1)}, f32[2,512]{1,0:T(2,128)S(1)}, s32[]{:T(128)}, s32[]{:T(128)}, /*index=5*/bf16[2048,128]{1,0:T(8,...) while((s32[]{:T(128)}, f32[512,2,64]{0,2,1:T(8,128)S(1)}, ...), condition=%wide.region_10.11_spmd.clone, body=%wide.region_6.10_spmd.clone.sunk | while | flops 439489024 | bytes 84838688 | solution.py:123
  73.6 5.1 %fusion.152 = (f32[2,512]{1,0:T(2,128)S(1)}, f32[2,512,1024]{1,2,0:T(8,128)S(1)}, f32[2,1024,512]{2,1,0:T(8,128)}) fusion(f32[2,1024]{1,0:T(2,128)S(1)} %dynamic-slice_convert_fusion.3, pred[512,1024]{0,1:T(8,128)(4,1)S(1)} %compare_and_fusion.2, bf16[1024,2,64]{0,2,1:T(8,128)(2,1)S(1)} %bitcast.133, bf16[512,2,64]{0,2,1:T(8,128)(2,1)S(1)} %get-tuple-element.278), kind=kOutput, calls=%fused_computation.33.clone.1 | convolution fusion | flops 145751040 | bytes 9318400 | tf_op jit(solution)/shard_map/while/body/qhd,khd->hqk/dot_general | solution.py:84
  78.7 10.1 %fusion.153 = f32[2,512,8,128]{1,2,3,0:T(8,128)S(1)} fusion(f32[2,512,8,128]{1,3,2,0:T(8,128)S(1)} %bitcast.131), kind=kOutput, calls=%fused_computation.19.clone.1 | output fusion | flops 133169152 | bytes 8388608 | tf_op jit(solution)/shard_map/reduce-window
  88.8 2.0 copy-done
  90.8 2.7 %broadcast_add_fusion.2 = f32[2,512,8,128]{1,2,3,0:T(8,128)S(1)} fusion(f32[2,512,8,128]{1,2,3,0:T(8,128)} %copy-done, f32[2,512,8]{1,2,0:T(8,128)S(1)} %slice.847), kind=kLoop, calls=%fused_computation.22.clone.1 | loop fusion | flops 1048576 | bytes 8421376 | tf_op jit(solution)/shard_map/reduce_window_sum | solution.py:91
  93.6 2.4 %copy.38 = f32[2,512,8,128]{1,3,2,0:T(8,128)S(1)} copy(f32[2,512,8,128]{1,2,3,0:T(8,128)S(1)} %broadcast_add_fusion.2) | data formatting | bytes 8388608 | tf_op jit(solution)/shard_map/reduce_window_sum | solution.py:91
  96.0 6.9 %fusion.154 = bf16[2,512,1024]{1,2,0:T(8,128)(2,1)S(1)} fusion(f32[2,512,8,128]{1,3,2,0:T(8,128)S(1)} %copy.38, f32[2,1024,512]{2,1,0:T(8,128)S(1)} %copy-done.1, f32[2,512]{1,0:T(2,128)S(1)} %get-tuple-element.258, f32[2,1024]{1,0:T(2,128)S(1)} %dynamic-slice_convert_fusion.3, pred[512,1024]{0,1:T(8,128)(4,1)S(1)} %compare_and_fusion.2), kind=kLoop, calls=%fused_computation.7.clone.1 | loop fusion | flops 24117248 | bytes 11022336 | tf_op jit(solution)/shard_map/while/body/convert_element_type | solution.py:92
  104.7 5.1 %fusion.152 = (f32[2,512]{1,0:T(2,128)S(1)}, f32[2,512,1024]{1,2,0:T(8,128)S(1)}, f32[2,1024,512]{2,1,0:T(8,128)}) fusion(f32[2,1024]{1,0:T(2,128)S(1)} %dynamic-slice_convert_fusion.3, pred[512,1024]{0,1:T(8,128)(4,1)S(1)} %compare_and_fusion.2, bf16[1024,2,64]{0,2,1:T(8,128)(2,1)S(1)} %bitcast.133, bf16[512,2,64]{0,2,1:T(8,128)(2,1)S(1)} %get-tuple-element.278), kind=kOutput, calls=%fused_computation.33.clone.1 | convolution fusion | flops 145751040 | bytes 9318400 | tf_op jit(solution)/shard_map/while/body/qhd,khd->hqk/dot_general | solution.py:84
  109.7 10.1 %fusion.153 = f32[2,512,8,128]{1,2,3,0:T(8,128)S(1)} fusion(f32[2,512,8,128]{1,3,2,0:T(8,128)S(1)} %bitcast.131), kind=kOutput, calls=%fused_computation.19.clone.1 | output fusion | flops 133169152 | bytes 8388608 | tf_op jit(solution)/shard_map/reduce-window
  119.8 2.0 copy-done
  121.9 2.7 %broadcast_add_fusion.2 = f32[2,512,8,128]{1,2,3,0:T(8,128)S(1)} fusion(f32[2,512,8,128]{1,2,3,0:T(8,128)} %copy-done, f32[2,512,8]{1,2,0:T(8,128)S(1)} %slice.847), kind=kLoop, calls=%fused_computation.22.clone.1 | loop fusion | flops 1048576 | bytes 8421376 | tf_op jit(solution)/shard_map/reduce_window_sum | solution.py:91
  124.6 2.4 %copy.38 = f32[2,512,8,128]{1,3,2,0:T(8,128)S(1)} copy(f32[2,512,8,128]{1,2,3,0:T(8,128)S(1)} %broadcast_add_fusion.2) | data formatting | bytes 8388608 | tf_op jit(solution)/shard_map/reduce_window_sum | solution.py:91
  127.0 6.9 %fusion.154 = bf16[2,512,1024]{1,2,0:T(8,128)(2,1)S(1)} fusion(f32[2,512,8,128]{1,3,2,0:T(8,128)S(1)} %copy.38, f32[2,1024,512]{2,1,0:T(8,128)S(1)} %copy-done.1, f32[2,512]{1,0:T(2,128)S(1)} %get-tuple-element.258, f32[2,1024]{1,0:T(2,128)S(1)} %dynamic-slice_convert_fusion.3, pred[512,1024]{0,1:T(8,128)(4,1)S(1)} %compare_and_fusion.2), kind=kLoop, calls=%fused_computation.7.clone.1 | loop fusion | flops 24117248 | bytes 11022336 | tf_op jit(solution)/shard_map/while/body/convert_element_type | solution.py:92
  136.0 1.5 collective-permute-start
  138.3 2.2 %collective-permute-done = f32[30,128]{1,0:T(8,128)S(1)} collective-permute-done((f32[30,128]{1,0:T(8,128)S(1)}, f32[30,128]{1,0:T(8,128)S(1)}, u32[]{:S(2)}, u32[]{:S(2)}) %collective-permute-start) | collective-permute-done | bytes 15392 | tf_op jit(solution)/shard_map/ppermute | solution.py:15
  141.6 17.4 %all-reduce = (f32[512]{0:T(512)S(1)}, f32[512]{0:T(512)S(1)}) all-reduce(f32[512]{0:T(512)S(1)} %get-tuple-element.104, f32[512]{0:T(512)S(1)} %get-tuple-element.103), channel_id=1, replica_groups=mesh['sp'=4,'fs'=4,'tp'=2] {'fs','tp'}, use_global_device_ids=true, to_apply=%region_4.0 | all-reduce | flops 1024 | bytes 8192 | tf_op jit(solution)/shard_map/psum | solution.py:65
  159.9 3.7 %all-gather.8.cloned.1.call-done = bf16[512,1024]{0,1:T(8,128)(2,1)} async-done(((bf16[512,128]{0,1:T(8,128)(2,1)}), bf16[512,1024]{0,1:T(8,128)(2,1)}) %all-gather.8.cloned.1.call-update) | async-done | bytes 1048592 | tf_op jit(solution)/shard_map/all_gather | solution.py:126
  163.6 1.5 fusion.23
  165.1 2.0 %convolution_multiply_fusion = f32[512,256]{1,0:T(8,128)S(1)} fusion(bf16[512,1024]{0,1:T(8,128)(2,1)} %all-gather.8.cloned.1.call-done, f32[1024]{0:T(1024)S(1)} %copy-done.5, bf16[2048,256]{1,0:T(8,128)(2,1)} %param.27, f32[512]{0:T(512)S(1)} %add_rsqrt_fusion), kind=kOutput, calls=%fused_computation.79 | convolution fusion | flops 270139392 | bytes 2103296 | tf_op jit(solution)/shard_map/dot_general | solution.py:135
  167.2 21.8 %all-gather.6.cloned.1.call-done = bf16[512,1024]{1,0:T(8,128)(2,1)} async-done(((bf16[512,128]{1,0:T(8,128)(2,1)}), bf16[512,1024]{1,0:T(8,128)(2,1)}) %all-gather.6.cloned.1.call-update) | async-done | bytes 1048592 | tf_op jit(solution)/shard_map/all_gather | solution.py:125
  189.0 1.5 fusion.21
  190.5 2.4 %fusion.34 = bf16[512,256]{1,0:T(8,128)(2,1)} fusion(f32[512,256]{1,0:T(8,128)S(1)} %convolution_multiply_fusion, bf16[512,1024]{1,0:T(8,128)(2,1)} %all-gather.6.cloned.1.call-done, f32[1024]{0:T(1024)S(1)} %copy-done.6, bf16[2048,256]{1,0:T(8,128)(2,1)S(1)} %copy-done.3, f32[512]{0:T(512)S(1)} %add_rsqrt_fusion.1), kind=kOutput, calls=%fused_computation.82 | convolution fusion | flops 270401536 | bytes 2365440 | tf_op jit(solution)/shard_map/dot_general | solution.py:134
  (66 shorter events, 9.7 us)
Async XLA Ops:
  6.5 17.0 %copy-start.2 = (bf16[2048,128]{1,0:T(8,128)(2,1)S(1)}, bf16[2048,128]{1,0:T(8,128)(2,1)}, u32[]{:S(2)}) copy-start(bf16[2048,128]{1,0:T(8,128)(2,1)} %param.21) | copy-start | bytes 1572868
  6.5 34.3 %copy-start.4 = (f32[2048]{0:T(1024)S(1)}, f32[2048]{0:T(1024)}, u32[]{:S(2)}) copy-start(f32[2048]{0:T(1024)} %param.16) | copy-start | bytes 24580
  6.5 32.2 %all-gather.4.cloned.1.call-start = ((), (), s32[]{:S(2)}) async-start(), calls=%async_computation | async-start | bytes 2359296 | tf_op jit(solution)/shard_map/all_gather | solution.py:43
  7.3 156.3 %all-gather.8.cloned.1.call-start = ((), (), s32[]{:S(2)}) async-start(), calls=%async_computation.2 | async-start | bytes 1179648 | tf_op jit(solution)/shard_map/all_gather | solution.py:126
  72.2 93.0 %copy-start.5 = (f32[1024]{0:T(1024)S(1)}, f32[1024]{0:T(1024)}, u32[]{:S(2)}) copy-start(f32[1024]{0:T(1024)} %param.26) | copy-start | bytes 12292
  88.8 2.0 copy-start
  93.6 2.4 %copy-start.1 = (f32[2,1024,512]{2,1,0:T(8,128)S(1)}, f32[2,1024,512]{2,1,0:T(8,128)}, u32[]{:S(2)}) copy-start(f32[2,1024,512]{2,1,0:T(8,128)} %get-tuple-element.239) | copy-start | bytes 12582916 | tf_op jit(solution)/shard_map/while
  119.8 2.0 copy-start
  124.6 2.4 %copy-start.1 = (f32[2,1024,512]{2,1,0:T(8,128)S(1)}, f32[2,1024,512]{2,1,0:T(8,128)}, u32[]{:S(2)}) copy-start(f32[2,1024,512]{2,1,0:T(8,128)} %get-tuple-element.239) | copy-start | bytes 12582916 | tf_op jit(solution)/shard_map/while
  134.4 56.1 %copy-start.3 = (bf16[2048,256]{1,0:T(8,128)(2,1)S(1)}, bf16[2048,256]{1,0:T(8,128)(2,1)}, u32[]{:S(2)}) copy-start(bf16[2048,256]{1,0:T(8,128)(2,1)} %param.27) | copy-start | bytes 3145732
  134.4 56.1 %copy-start.6 = (f32[1024]{0:T(1024)S(1)}, f32[1024]{0:T(1024)}, u32[]{:S(2)}) copy-start(f32[1024]{0:T(1024)} %param.25) | copy-start | bytes 12292
  135.2 53.8 %all-gather.6.cloned.1.call-start = ((), (), s32[]{:S(2)}) async-start(), calls=%async_computation.1 | async-start | bytes 1179648 | tf_op jit(solution)/shard_map/all_gather | solution.py:125
  136.0 4.5 %collective-permute-start = (f32[30,128]{1,0:T(8,128)S(1)}, f32[30,128]{1,0:T(8,128)S(1)}, u32[]{:S(2)}, u32[]{:S(2)}) collective-permute-start(f32[30,128]{1,0:T(8,128)S(1)} %slice.285), channel_id=1, source_target_pairs={{0,8},{8,16},{16,24},{1,9},{9,17},{17,25},{2,10},{10,18},{18,26},{... | collective-permute-start | bytes 46088 | tf_op jit(solution)/shard_map/ppermute | solution.py:15
Sparse Core Ops, SparseCore 0:
  9.2 29.4 all-gather.3
  135.3 28.2 all-gather.7
  165.5 23.4 all-gather.5
where the time goes:
time: 201 us; the launch traced here: 199 us
  blocking collectives  52.8 us (26%)
  other arithmetic  49.7 us (25%)
  waiting for transfers between devices  42.8 us (21%)
  matrix products  19.7 us (10%)
  local copies, waits for them, and re-layouts  19.1 us (10%)
  between operations  13.3 us (7%)
    all_gather x1, waiting for transfers between devices, per_device(): conv_piece = lax.all_gather(conv_mixed, ('fs', 'tp'), axis=1, tiled=True)  21.8 us
    another operation x4, other arithmetic  20.3 us
    psum x1, blocking collectives, per_device(): lax.psum((jnp.sum(conv_out, axis=1), jnp.sum(conv_out * conv_out, axis=1)...  17.4 us
    all_gather x1, waiting for transfers between devices, per_device(): segment = lax.all_gather(tokens, ('fs', 'tp'), axis=1, tiled=True)  14.4 us
    convert_element_type x2, other arithmetic, attend(): jnp.where(allowed, jnp.exp(jax.nn.log_sigmoid(scores) + later_sum), 0.0)  13.7 us
    all_gather x1, blocking collectives, per_device(): lax.all_gather(key, 'sp', axis=0, tiled=True)  13.7 us
    all_gather x1, blocking collectives, per_device(): lax.all_gather(value, 'sp', axis=0, tiled=True)  13.2 us
    dot_general x2, matrix products, attend(): jnp.einsum('qhd,khd->hqk', queries, key_heads, preferred_element_type=jnp...  10.1 us
  transfers between devices with their start and end apart: 4, of which 4 were waited for; matrix products, arithmetic and copies ran while one was open for 8% of the time, Pallas kernels for 0%

commit v1 on v0

v1 whole, which is shorter than its diff:
```python
import functools
import math

import jax
import jax.numpy as jnp
from jax import lax
from jax.experimental import pallas as pl
from jax.experimental.pallas import tpu as pltpu
from jax.sharding import PartitionSpec as P

HEAD_DIM = 64
LANES = 128
KEY_TILE = 256
HALO = 32
LOG2E = math.log2(math.e)
MESH = pl.DeviceIdType.MESH
F32 = jnp.float32
BF16 = jnp.bfloat16

epsilon = 1e-06


def dot_tt(left, right, precision=None):
    return lax.dot_general(
        left, right, (((1,), (1,)), ((), ())), precision=precision, preferred_element_type=F32
    )


def layer_kernel(
    nsp,
    nfs,
    ntp,
    tokens,
    w_a,
    w_gate,
    w_q,
    w_k,
    w_v,
    w_out,
    in_gain,
    taps,
    norm_gain,
    shift,
    conv_gain,
    attn_gain,
    out,
    xbuf,
    wbuf,
    wout,
    acc,
    squares,
    qbuf,
    kvbuf,
    shbuf,
    gbuf,
    convbuf,
    tri,
    stat,
    own_conv,
    own_attn,
    cbuf,
    abuf,
    obuf,
    behind,
    local_sem,
    tok_send,
    tok_recv,
    tokp_send,
    tokp_recv,
    att_send,
    att_recv,
    attp_send,
    attp_recv,
    kv_send,
    kv_recv,
    sh_send,
    sh_recv,
    halo_sem,
    stat_send,
    stat_recv,
    conv_send,
    conv_recv,
):
    s = lax.axis_index("sp")
    f = lax.axis_index("fs")
    c = lax.axis_index("tp")
    group = nfs * ntp
    g = f * ntp + c
    rows = tokens.shape[0]
    cols = tokens.shape[1]
    width = w_a.shape[1]
    heads = shift.shape[0]
    channels = width * group
    model = cols * group

    def in_group(index):
        return {"fs": index // ntp, "tp": lax.rem(index, ntp)}

    barrier = pltpu.get_barrier_semaphore()
    for d in range(1, group):
        pl.semaphore_signal(
            barrier, inc=1, device_id=in_group(lax.rem(g + d, group)), device_id_type=MESH
        )

    def greet(d, carry):
        pl.semaphore_signal(
            barrier, inc=1, device_id={"sp": lax.rem(s + d, nsp)}, device_id_type=MESH
        )
        return carry

    lax.fori_loop(1, nsp, greet, 0)

    locals_ = [pltpu.make_async_copy(tokens, xbuf.at[g], local_sem.at[0])]
    for i, w in enumerate((w_a, w_gate, w_q, w_k, w_v)):
        locals_.append(
            pltpu.make_async_copy(
                w, wbuf.at[:, pl.ds(i * width, width)], local_sem.at[1 + i]
            )
        )
    locals_.append(pltpu.make_async_copy(w_out, wout, local_sem.at[6]))
    for copy in locals_:
        copy.start()

    shbuf[0] = jnp.zeros(shbuf.shape[1:], F32)
    shbuf[0, pl.ds(0, heads), :] = shift[...].astype(F32) * LOG2E
    ki = lax.broadcasted_iota(jnp.int32, (KEY_TILE, KEY_TILE), 0)
    kj = lax.broadcasted_iota(jnp.int32, (KEY_TILE, KEY_TILE), 1)
    tri[...] = (ki >= kj).astype(F32).astype(BF16)

    pl.semaphore_wait(barrier, group - 1 + nsp - 1)

    def direct(src, dst, send, recv, k):
        return pltpu.make_async_remote_copy(
            src_ref=src,
            dst_ref=dst,
            send_sem=send.at[k],
            recv_sem=recv.at[k],
            device_id={"fs": lax.rem(f + k, nfs)},
            device_id_type=MESH,
        )

    def partner(src, dst, send, recv, m, k):
        return pltpu.make_async_remote_copy(
            src_ref=src,
            dst_ref=dst,
            send_sem=send.at[m, k],
            recv_sem=recv.at[m, k],
            device_id={"tp": lax.rem(c + m, ntp)},
            device_id_type=MESH,
        )

    def chip_from(k):
        return lax.rem(f + nfs - k, nfs)

    def gather(own, buf, sems, consume):
        send, recv, psend, precv = sems
        sent = []
        for k in range(1, nfs):
            copy = direct(own, buf.at[g], send, recv, k)
            copy.start()
            sent.append(copy)
        for m in range(1, ntp):
            copy = partner(own, buf.at[g], psend, precv, m, 0)
            copy.start()
            sent.append(copy)
        consume(g, True)
        for m in range(1, ntp):
            origin = f * ntp + lax.rem(c + ntp - m, ntp)
            partner(own, buf.at[origin], psend, precv, m, 0).wait_recv()
            consume(origin, False)
        for k in range(1, nfs):
            origin = chip_from(k) * ntp + c
            direct(own, buf.at[origin], send, recv, k).wait_recv()
            for m in range(1, ntp):
                copy = partner(buf.at[origin], buf.at[origin], psend, precv, m, k)
                copy.start()
                sent.append(copy)
            consume(origin, False)
        for k in range(1, nfs):
            for m in range(1, ntp):
                origin = chip_from(k) * ntp + lax.rem(c + ntp - m, ntp)
                partner(own, buf.at[origin], psend, precv, m, k).wait_recv()
                consume(origin, False)
        return sent

    def send_shift(d, carry):
        pltpu.make_async_remote_copy(
            src_ref=shbuf.at[0],
            dst_ref=shbuf.at[d],
            send_sem=sh_send.at[d],
            recv_sem=sh_recv.at[d],
            device_id={"sp": s + d},
            device_id_type=MESH,
        ).start()
        return carry

    def project(index, first):
        if first:
            for copy in locals_[:6]:
                copy.wait()
        x = xbuf[index].astype(F32)
        per = cols // LANES
        gain = jnp.concatenate(
            [in_gain[pl.ds(index * per + j, 1), :] for j in range(per)], axis=1
        )
        scaled = (x * gain).astype(BF16)
        w = wbuf[pl.ds(pl.multiple_of(index * cols, cols), cols), :]
        part = jnp.dot(scaled, w, preferred_element_type=F32)
        sq = x * x
        folded = sq[:, :LANES]
        for j in range(1, per):
            folded = folded + sq[:, j * LANES : (j + 1) * LANES]
        if first:
            acc[...] = part
            squares[...] = folded
        else:
            acc[...] += part
            squares[...] += folded

    sent = gather(tokens, xbuf, (tok_send, tok_recv, tokp_send, tokp_recv), project)
    lax.fori_loop(1, nsp - s, send_shift, 0)

    scale = lax.rsqrt(jnp.sum(squares[...], axis=1, keepdims=True) / model + epsilon)

    def projected(i):
        return (acc[:, i * width : (i + 1) * width] * scale).astype(BF16)

    kvbuf[0, :, :width] = projected(3)
    kvbuf[0, :, width:] = projected(4)

    a = projected(0).astype(F32)
    gate = projected(1).astype(F32)
    gbuf[pl.ds(HALO, rows), :] = a / (1.0 + jnp.exp(-gate))

    def kv_copy(d):
        return pltpu.make_async_remote_copy(
            src_ref=kvbuf.at[0],
            dst_ref=kvbuf.at[d],
            send_sem=kv_send.at[d],
            recv_sem=kv_recv.at[d],
            device_id={"sp": lax.rem(s + d, nsp)},
            device_id_type=MESH,
        )

    def sh_copy(d):
        return pltpu.make_async_remote_copy(
            src_ref=shbuf.at[0],
            dst_ref=shbuf.at[d],
            send_sem=sh_send.at[d],
            recv_sem=sh_recv.at[d],
            device_id={"sp": lax.rem(s + d, nsp)},
            device_id_type=MESH,
        )

    halo = pltpu.make_async_remote_copy(
        src_ref=gbuf.at[pl.ds(rows, HALO)],
        dst_ref=gbuf.at[pl.ds(0, HALO)],
        send_sem=halo_sem.at[0],
        recv_sem=halo_sem.at[1],
        device_id={"sp": lax.rem(s + 1, nsp)},
        device_id_type=MESH,
    )

    @pl.when(s + 1 < nsp)
    def _():
        halo.start()

    def send_kv(d, carry):
        kv_copy(d).start()
        return carry

    lax.fori_loop(1, nsp - s, send_kv, 0)

    lane = lax.broadcasted_iota(jnp.int32, (1, width), 1)
    head_lanes = [
        ((lane >= h * HEAD_DIM) & (lane < (h + 1) * HEAD_DIM)).astype(F32) for h in range(heads)
    ]
    q = projected(2).astype(F32) * (HEAD_DIM**-0.5)
    for h in range(heads):
        qbuf[h] = (q * head_lanes[h]).astype(BF16)
    obuf[...] = jnp.zeros_like(obuf)
    behind[...] = jnp.zeros_like(behind)

    def tile(slot, h, row0, count, key0, masked):
        rs = pl.ds(row0, count)
        keys = kvbuf[slot, pl.ds(key0, KEY_TILE), :width]
        values = kvbuf[slot, pl.ds(key0, KEY_TILE), width:]
        values = (values.astype(F32) * head_lanes[h]).astype(BF16)
        shifts = shbuf[slot, pl.ds(h, 1), pl.ds(key0, KEY_TILE)]
        scores = dot_tt(qbuf[h, rs, :], keys) * LOG2E + shifts
        fail = jnp.maximum(scores, 0.0) + LOG2E * jnp.log(1.0 + jnp.exp2(-jnp.abs(scores)))
        if masked:
            qi = row0 + lax.broadcasted_iota(jnp.int32, (count, KEY_TILE), 0)
            kk = key0 + lax.broadcasted_iota(jnp.int32, (count, KEY_TILE), 1)
            allowed = kk < qi
            fail = jnp.where(allowed, fail, 0.0)
        high = fail.astype(BF16)
        low = (fail - high.astype(F32)).astype(BF16)
        sums = jnp.dot(high, tri[...], preferred_element_type=F32) + jnp.dot(
            low, tri[...], preferred_element_type=F32
        )
        past = behind[h, rs, :]
        past_wide = jnp.concatenate([past] * (KEY_TILE // LANES), axis=1)
        weights = jnp.exp2(scores - sums - past_wide)
        if masked:
            weights = jnp.where(allowed, weights, 0.0)
        obuf[rs, :] += jnp.dot(weights.astype(BF16), values, preferred_element_type=F32)
        behind[h, rs, :] = past + sums[:, :1]

    tiles = rows // KEY_TILE
    for h in range(heads):
        for qt in range(tiles):
            for kt in range(qt, -1, -1):
                tile(0, h, qt * KEY_TILE, KEY_TILE, kt * KEY_TILE, kt == qt)

    @pl.when(s == 0)
    def _():
        gbuf[pl.ds(0, HALO), :] = jnp.zeros((HALO, width), F32)

    @pl.when(s > 0)
    def _():
        halo.wait_recv()

    ntaps = taps.shape[0]
    tap = taps[:, pl.ds(pl.multiple_of(g * width, width), width)].astype(F32)
    chunk = 128
    for r0 in range(0, rows, chunk):
        total = jnp.zeros((chunk, width), F32)
        for j in range(ntaps):
            first = r0 + j + HALO - (ntaps - 1)
            total = total + tap[j : j + 1, :] * gbuf[pl.ds(first, chunk), :]
        convbuf[pl.ds(r0, chunk), :] = total

    conv = convbuf[...]
    ones = jnp.ones((8, width), F32)
    sub = lax.broadcasted_iota(jnp.int32, (8, rows), 0)
    hp = lax.Precision.HIGHEST
    stat[0] = jnp.where(sub == 0, dot_tt(ones, conv, hp), dot_tt(ones, conv * conv, hp))

    def stat_copy(d):
        return pltpu.make_async_remote_copy(
            src_ref=stat.at[0],
            dst_ref=stat.at[d],
            send_sem=stat_send.at[d],
            recv_sem=stat_recv.at[d],
            device_id=in_group(lax.rem(g + d, group)),
            device_id_type=MESH,
        )

    for d in range(1, group):
        stat_copy(d).start()
    totals = stat[0]
    for d in range(1, group):
        stat_copy(d).wait_recv()
        totals = totals + stat[d]
    pick = lax.broadcasted_iota(jnp.int32, (8, width), 0)
    turned = (((0,), (0,)), ((), ()))
    first_sum = lax.dot_general(
        totals, (pick == 0).astype(F32), turned, precision=hp, preferred_element_type=F32
    )
    second_sum = lax.dot_general(
        totals, (pick == 1).astype(F32), turned, precision=hp, preferred_element_type=F32
    )
    mean = first_sum / channels
    spread = jnp.maximum(second_sum / channels - mean * mean, 0.0)
    normed = (conv - mean) * lax.rsqrt(spread + epsilon) * norm_gain[pl.ds(g, 1), :]
    mixed = (normed / (1.0 + jnp.exp(-normed))).astype(BF16)
    own_conv[...] = mixed
    cbuf[g] = mixed

    def conv_copy(d, index):
        return pltpu.make_async_remote_copy(
            src_ref=own_conv,
            dst_ref=cbuf.at[index],
            send_sem=conv_send.at[d],
            recv_sem=conv_recv.at[d],
            device_id=in_group(lax.rem(g + d, group)),
            device_id_type=MESH,
        )

    for d in range(1, group):
        conv_copy(d, g).start()

    def attend(d, carry):
        sh_copy(d).wait_recv()
        kv_copy(d).wait_recv()
        for h in range(heads):
            for kt in range(tiles - 1, -1, -1):
                tile(d, h, 0, rows, kt * KEY_TILE, False)
        return carry

    lax.fori_loop(1, s + 1, attend, 0)

    attn = obuf[...].astype(BF16)
    own_attn[...] = attn
    abuf[g] = attn

    locals_[6].wait()

    def mix(buf, gain, base, index, first):
        v = buf[index].astype(F32)
        scaled = (v * gain[pl.ds(index, 1), :]).astype(BF16)
        w = wout[pl.ds(pl.multiple_of(base + index * width, width), width), :]
        part = jnp.dot(scaled, w, preferred_element_type=F32)
        if first:
            acc[:, : out.shape[1]] = part
            squares[...] = v * v
        else:
            acc[:, : out.shape[1]] += part
            squares[...] += v * v

    def mix_conv():
        mix(cbuf, conv_gain, 0, g, True)
        for d in range(1, group):
            origin = lax.rem(g + group - d, group)
            conv_copy(d, origin).wait_recv()
            mix(cbuf, conv_gain, 0, origin, False)
        conv_scale = lax.rsqrt(
            jnp.sum(squares[...], axis=1, keepdims=True) / channels + epsilon
        )
        out_width = out.shape[1]
        acc[:, out_width : 2 * out_width] = acc[:, :out_width] * conv_scale

    def mix_attn(index, first):
        if first:
            mix_conv()
        mix(abuf, attn_gain, channels, index, first)

    sent += gather(own_attn, abuf, (att_send, att_recv, attp_send, attp_recv), mix_attn)
    out_width = out.shape[1]
    attn_scale = lax.rsqrt(jnp.sum(squares[...], axis=1, keepdims=True) / channels + epsilon)
    out[...] = (acc[:, out_width : 2 * out_width] + acc[:, :out_width] * attn_scale).astype(BF16)

    for copy in sent:
        copy.wait_send()
    for d in range(1, group):
        stat_copy(d).wait_send()
        conv_copy(d, g).wait_send()

    @pl.when(s + 1 < nsp)
    def _():
        halo.wait_send()

    def finish(d, carry):
        sh_copy(d).wait_send()
        kv_copy(d).wait_send()
        return carry

    lax.fori_loop(1, nsp - s, finish, 0)


def per_device(
    tokens,
    in_gain,
    conv_a_weight,
    conv_gate_weight,
    query_weight,
    key_weight,
    value_weight,
    conv_taps,
    conv_norm_gain,
    break_shift,
    conv_out_gain,
    attn_out_gain,
    out_weight,
):
    nsp, nfs, ntp = (lax.axis_size(axis) for axis in ("sp", "fs", "tp"))
    group = nfs * ntp
    rows, cols = tokens.shape
    model = in_gain.shape[0]
    width = conv_a_weight.shape[1]
    heads = break_shift.shape[0]
    out_width = out_weight.shape[1]
    vm = pl.BlockSpec(memory_space=pltpu.VMEM)
    hbm = pl.BlockSpec(memory_space=pl.ANY)
    dma = pltpu.SemaphoreType.DMA
    return pl.pallas_call(
        functools.partial(layer_kernel, nsp, nfs, ntp),
        out_shape=jax.ShapeDtypeStruct((rows, out_width), BF16),
        in_specs=[hbm] * 7 + [vm] * 6,
        out_specs=vm,
        scratch_shapes=[
            pltpu.VMEM((group, rows, cols), BF16),
            pltpu.VMEM((model, 5 * width), BF16),
            pltpu.VMEM((model, out_width), BF16),
            pltpu.VMEM((rows, 5 * width), F32),
            pltpu.VMEM((rows, LANES), F32),
            pltpu.VMEM((heads, rows, width), BF16),
            pltpu.VMEM((nsp, rows, 2 * width), BF16),
            pltpu.VMEM((nsp, 8, rows), F32),
            pltpu.VMEM((HALO + rows, width), F32),
            pltpu.VMEM((rows, width), F32),
            pltpu.VMEM((KEY_TILE, KEY_TILE), BF16),
            pltpu.VMEM((group, 8, rows), F32),
            pltpu.VMEM((rows, width), BF16),
            pltpu.VMEM((rows, width), BF16),
            pltpu.VMEM((group, rows, width), BF16),
            pltpu.VMEM((group, rows, width), BF16),
            pltpu.VMEM((rows, width), F32),
            pltpu.VMEM((heads, rows, LANES), F32),
            dma((7,)),
            dma((nfs,)),
            dma((nfs,)),
            dma((ntp, nfs)),
            dma((ntp, nfs)),
            dma((nfs,)),
            dma((nfs,)),
            dma((ntp, nfs)),
            dma((ntp, nfs)),
            dma((nsp,)),
            dma((nsp,)),
            dma((nsp,)),
            dma((nsp,)),
            dma((2,)),
            dma((group,)),
            dma((group,)),
            dma((group,)),
            dma((group,)),
        ],
        compiler_params=pltpu.CompilerParams(
            collective_id=0, has_side_effects=True, vmem_limit_bytes=48 * 2**20
        ),
        name="layer",
    )(
        tokens,
        conv_a_weight,
        conv_gate_weight,
        query_weight,
        key_weight,
        value_weight,
        out_weight,
        in_gain.reshape(-1, LANES),
        conv_taps,
        conv_norm_gain.reshape(-1, LANES),
        break_shift,
        conv_out_gain.reshape(-1, LANES),
        attn_out_gain.reshape(-1, LANES),
    )


def solution(mesh):
    split = P(None, ("fs", "tp"))
    return jax.shard_map(
        per_device,
        mesh=mesh,
        in_specs=(
            P("sp", ("fs", "tp")),
            P(),
            split,
            split,
            split,
            split,
            split,
            P(),
            P(),
            P(("fs", "tp"), "sp"),
            P(),
            P(),
            split,
        ),
        out_specs=P("sp", ("fs", "tp")),
        check_vma=False,
    )
```

time: 201 us -> 71.8 us (0.36)
  Pallas kernels: 0 us -> 59.5 us
  blocking collectives: 52.8 us -> 0 us
  other arithmetic: 49.7 us -> 0 us
  waiting for transfers between devices: 42.8 us -> 0 us
  matrix products: 19.7 us -> 0 us
  between operations: 13.3 us -> 0.02 us
  local copies, waits for them, and re-layouts: 19.1 us -> 11.7 us
    pallas_call x0 -> x1, Pallas kernels: none -> 59.5 us  [per_device(): pl.pallas_call(functools.partial(layer_kernel, nsp, nfs, ntp), out_shape=...]
    all_gather x3 -> x0, waiting for transfers between devices: 39.9 us -> none  [the longest x1 21.8 us: per_device(): conv_piece = lax.all_gather(conv_mixed, ('fs', 'tp'), axis=1, tiled=True)]
    all_gather x3 -> x0, blocking collectives: 35.4 us -> none  [the longest x1 13.7 us: per_device(): lax.all_gather(key, 'sp', axis=0, tiled=True)]
    another operation x6 -> x0, other arithmetic: 25.7 us -> none
    dot_general x7 -> x0, matrix products: 19.7 us -> none  [the longest x2 10.1 us: attend(): jnp.einsum('qhd,khd->hqk', queries, key_heads, preferred_element_type=jnp...]
    psum x1 -> x0, blocking collectives: 17.4 us -> none  [per_device(): lax.psum((jnp.sum(conv_out, axis=1), jnp.sum(conv_out * conv_out, axis=1)...]
    convert_element_type x7 -> x0, other arithmetic: 16 us -> none  [the longest x2 13.7 us: attend(): jnp.where(allowed, jnp.exp(jax.nn.log_sigmoid(scores) + later_sum), 0.0)]
    reduce_sum x4 -> x0, other arithmetic: 6.14 us -> none  [the longest x1 2.07 us: per_device(): totals, squares = (totals, jnp.sum(segment_wide * segment_wide, axis=1))]
  transfers between devices with their start and end apart: 4 -> 0, of which waited for: 4 -> 0; matrix products, arithmetic and copies ran while one was open for 8% -> 0% of each run, Pallas kernels for 0% -> 0%
where the time goes in v1:
time: 71.8 us; the launch traced here: 71.2 us
  Pallas kernels  59.5 us (83%)
  local copies, waits for them, and re-layouts  11.7 us (16%)
    pallas_call x1, Pallas kernels, per_device(): pl.pallas_call(functools.partial(layer_kernel, nsp, nfs, ntp), out_shape=...  59.5 us
    unnamed x27, local copies, waits for them, and re-layouts  11.7 us

profile of v1, /device:TPU:25, one launch (start us, length us, event | category | flops | bytes accessed | tf_op | source)
XLA Modules:
  0.0 71.2 jit_solution(6685240770179852707)
XLA Ops:
  0.0 0.0 copy-start.9
  0.0 0.0 copy-start.12
  0.0 0.7 copy-done.9
  0.7 0.0 copy-done.12
  0.7 0.0 copy-start
  0.7 1.2 %copy-done = bf16[2048,256]{1,0:T(8,128)(2,1)S(1)} copy-done((bf16[2048,256]{1,0:T(8,128)(2,1)S(1)}, bf16[2048,256]{1,0:T(8,128)(2,1)}, u32[]{:S(2)}) %copy-start) | copy-done | bytes 1048600
  1.9 0.0 copy-start.1
  1.9 1.0 %copy-done.1 = bf16[2048,128]{1,0:T(8,128)(2,1)S(1)} copy-done((bf16[2048,128]{1,0:T(8,128)(2,1)S(1)}, bf16[2048,128]{1,0:T(8,128)(2,1)}, u32[]{:S(2)}) %copy-start.1) | copy-done | bytes 524312
  3.0 0.0 copy-start.2
  3.0 1.0 %copy-done.2 = bf16[2048,128]{1,0:T(8,128)(2,1)S(1)} copy-done((bf16[2048,128]{1,0:T(8,128)(2,1)S(1)}, bf16[2048,128]{1,0:T(8,128)(2,1)}, u32[]{:S(2)}) %copy-start.2) | copy-done | bytes 524312
  4.0 0.0 copy-start.3
  4.0 1.0 %copy-done.3 = bf16[2048,128]{1,0:T(8,128)(2,1)S(1)} copy-done((bf16[2048,128]{1,0:T(8,128)(2,1)S(1)}, bf16[2048,128]{1,0:T(8,128)(2,1)}, u32[]{:S(2)}) %copy-start.3) | copy-done | bytes 524312
  5.0 0.0 copy-start.4
  5.1 1.0 %copy-done.4 = bf16[2048,128]{1,0:T(8,128)(2,1)S(1)} copy-done((bf16[2048,128]{1,0:T(8,128)(2,1)S(1)}, bf16[2048,128]{1,0:T(8,128)(2,1)}, u32[]{:S(2)}) %copy-start.4) | copy-done | bytes 524312
  6.1 0.0 copy-start.5
  6.1 1.0 %copy-done.5 = bf16[2048,128]{1,0:T(8,128)(2,1)S(1)} copy-done((bf16[2048,128]{1,0:T(8,128)(2,1)S(1)}, bf16[2048,128]{1,0:T(8,128)(2,1)}, u32[]{:S(2)}) %copy-start.5) | copy-done | bytes 524312
  7.1 0.0 copy-start.6
  7.1 0.9 %copy-done.6 = bf16[512,256]{1,0:T(8,128)(2,1)S(1)} copy-done((bf16[512,256]{1,0:T(8,128)(2,1)S(1)}, bf16[512,256]{1,0:T(8,128)(2,1)}, u32[]{:S(2)}) %copy-start.6) | copy-done | bytes 262168
  8.1 0.0 copy-start.7
  8.1 0.8 %copy-done.7 = bf16[31,1024]{1,0:T(8,128)(2,1)S(1)} copy-done((bf16[31,1024]{1,0:T(8,128)(2,1)S(1)}, bf16[31,1024]{1,0:T(8,128)(2,1)}, u32[]{:S(2)}) %copy-start.7) | copy-done | bytes 63512
  8.9 0.0 copy-start.8
  8.9 0.7 copy-done.8
  9.6 0.0 copy-start.10
  9.6 0.7 copy-done.10
  10.3 0.0 copy-start.11
  10.3 0.7 copy-done.11
  11.0 59.5 %layer.1 = bf16[512,256]{1,0:T(8,128)(2,1)S(1)} custom-call(bf16[512,256]{1,0:T(8,128)(2,1)S(1)} %copy-done.6, bf16[2048,128]{1,0:T(8,128)(2,1)S(1)} %copy-done.1, bf16[2048,128]{1,0:T(8,128)(2,1)S(1)} %copy-done.2, bf16[2048,128]{1,0:T(8,128)(2,1)S(1)} %copy-done.3, bf16[2048,128]{1,0:T(8,128)(2,1)S(1)} %copy-done.4, bf16[2048,128]{1,0:T(8,128)(2,1)S(1)} %copy-done.5, ...), custom_call_target="tpu_custom_call" | custom-call | tf_op jit(solution)/shard_map/layer/pallas_call | solution.py:477
  70.5 0.7 copy.15
Async XLA Ops:
  0.0 0.7 copy-start.9
  0.0 0.7 copy-start.12
  0.7 1.2 %copy-start = (bf16[2048,256]{1,0:T(8,128)(2,1)S(1)}, bf16[2048,256]{1,0:T(8,128)(2,1)}, u32[]{:S(2)}) copy-start(bf16[2048,256]{1,0:T(8,128)(2,1)} %w_out.1) | copy-start | bytes 3145732
  1.9 1.0 %copy-start.1 = (bf16[2048,128]{1,0:T(8,128)(2,1)S(1)}, bf16[2048,128]{1,0:T(8,128)(2,1)}, u32[]{:S(2)}) copy-start(bf16[2048,128]{1,0:T(8,128)(2,1)} %w_a.1) | copy-start | bytes 1572868
  3.0 1.0 %copy-start.2 = (bf16[2048,128]{1,0:T(8,128)(2,1)S(1)}, bf16[2048,128]{1,0:T(8,128)(2,1)}, u32[]{:S(2)}) copy-start(bf16[2048,128]{1,0:T(8,128)(2,1)} %w_gate.1) | copy-start | bytes 1572868
  4.0 1.0 %copy-start.3 = (bf16[2048,128]{1,0:T(8,128)(2,1)S(1)}, bf16[2048,128]{1,0:T(8,128)(2,1)}, u32[]{:S(2)}) copy-start(bf16[2048,128]{1,0:T(8,128)(2,1)} %w_q.1) | copy-start | bytes 1572868
  5.0 1.0 %copy-start.4 = (bf16[2048,128]{1,0:T(8,128)(2,1)S(1)}, bf16[2048,128]{1,0:T(8,128)(2,1)}, u32[]{:S(2)}) copy-start(bf16[2048,128]{1,0:T(8,128)(2,1)} %w_k.1) | copy-start | bytes 1572868
  6.1 1.0 %copy-start.5 = (bf16[2048,128]{1,0:T(8,128)(2,1)S(1)}, bf16[2048,128]{1,0:T(8,128)(2,1)}, u32[]{:S(2)}) copy-start(bf16[2048,128]{1,0:T(8,128)(2,1)} %w_v.1) | copy-start | bytes 1572868
  7.1 0.9 %copy-start.6 = (bf16[512,256]{1,0:T(8,128)(2,1)S(1)}, bf16[512,256]{1,0:T(8,128)(2,1)}, u32[]{:S(2)}) copy-start(bf16[512,256]{1,0:T(8,128)(2,1)} %tokens.1) | copy-start | bytes 786436
  8.1 0.8 %copy-start.7 = (bf16[31,1024]{1,0:T(8,128)(2,1)S(1)}, bf16[31,1024]{1,0:T(8,128)(2,1)}, u32[]{:S(2)}) copy-start(bf16[31,1024]{1,0:T(8,128)(2,1)} %taps.1) | copy-start | bytes 190468
  8.9 0.7 copy-start.8
  9.6 0.7 copy-start.10
  10.3 0.7 copy-start.11

commit v2 on v1

--- a/solution.py
+++ b/solution.py
@@ -80,6 +80,8 @@
     stat_recv,
     conv_send,
     conv_recv,
+    convp_send,
+    convp_recv,
 ):
     s = lax.axis_index("sp")
     f = lax.axis_index("fs")
@@ -133,18 +135,18 @@
         return pltpu.make_async_remote_copy(
             src_ref=src,
             dst_ref=dst,
-            send_sem=send.at[k],
-            recv_sem=recv.at[k],
+            send_sem=send,
+            recv_sem=recv,
             device_id={"fs": lax.rem(f + k, nfs)},
             device_id_type=MESH,
         )
 
-    def partner(src, dst, send, recv, m, k):
+    def partner(src, dst, send, recv, m):
         return pltpu.make_async_remote_copy(
             src_ref=src,
             dst_ref=dst,
-            send_sem=send.at[m, k],
-            recv_sem=recv.at[m, k],
+            send_sem=send,
+            recv_sem=recv,
             device_id={"tp": lax.rem(c + m, ntp)},
             device_id_type=MESH,
         )
@@ -152,36 +154,49 @@
     def chip_from(k):
         return lax.rem(f + nfs - k, nfs)
 
-    def gather(own, buf, sems, consume):
+    sent = []
+
+    def start(own, view, sems, base):
         send, recv, psend, precv = sems
-        sent = []
         for k in range(1, nfs):
-            copy = direct(own, buf.at[g], send, recv, k)
+            copy = direct(own, view(g), send.at[base + k], recv.at[base + k], k)
             copy.start()
             sent.append(copy)
         for m in range(1, ntp):
-            copy = partner(own, buf.at[g], psend, precv, m, 0)
+            copy = partner(own, view(g), psend.at[m, base], precv.at[m, base], m)
             copy.start()
             sent.append(copy)
-        consume(g, True)
-        for m in range(1, ntp):
-            origin = f * ntp + lax.rem(c + ntp - m, ntp)
-            partner(own, buf.at[origin], psend, precv, m, 0).wait_recv()
-            consume(origin, False)
+
+    def relay(own, view, sems, base, consume):
+        send, recv, psend, precv = sems
         for k in range(1, nfs):
             origin = chip_from(k) * ntp + c
-            direct(own, buf.at[origin], send, recv, k).wait_recv()
+            direct(own, view(origin), send.at[base + k], recv.at[base + k], k).wait_recv()
             for m in range(1, ntp):
-                copy = partner(buf.at[origin], buf.at[origin], psend, precv, m, k)
+                copy = partner(
+                    view(origin), view(origin), psend.at[m, base + k], precv.at[m, base + k], m
+                )
                 copy.start()
                 sent.append(copy)
-            consume(origin, False)
+            if consume is not None:
+                consume(origin)
+
+    def finish_relay(own, view, sems, base, consume):
+        send, recv, psend, precv = sems
         for k in range(1, nfs):
             for m in range(1, ntp):
                 origin = chip_from(k) * ntp + lax.rem(c + ntp - m, ntp)
-                partner(own, buf.at[origin], psend, precv, m, k).wait_recv()
-                consume(origin, False)
-        return sent
+                partner(
+                    own, view(origin), psend.at[m, base + k], precv.at[m, base + k], m
+                ).wait_recv()
+                consume(origin)
+
+    def own_chip(own, view, sems, base, consume):
+        send, recv, psend, precv = sems
+        for m in range(1, ntp):
+            origin = f * ntp + lax.rem(c + ntp - m, ntp)
+            partner(own, view(origin), psend.at[m, base], precv.at[m, base], m).wait_recv()
+            consume(origin)
 
     def send_shift(d, carry):
         pltpu.make_async_remote_copy(
@@ -194,11 +209,9 @@
         ).start()
         return carry
 
-    def project(index, first):
-        if first:
-            for copy in locals_[:6]:
-                copy.wait()
-        x = xbuf[index].astype(F32)
+    def project(index, row0, first):
+        rs = pl.ds(row0, KEY_TILE)
+        x = xbuf[index, rs, :].astype(F32)
         per = cols // LANES
         gain = jnp.concatenate(
             [in_gain[pl.ds(index * per + j, 1), :] for j in range(per)], axis=1
@@ -211,33 +224,19 @@
         for j in range(1, per):
             folded = folded + sq[:, j * LANES : (j + 1) * LANES]
         if first:
-            acc[...] = part
-            squares[...] = folded
+            acc[rs, :] = part
+            squares[rs, :] = folded
         else:
-            acc[...] += part
-            squares[...] += folded
-
-    sent = gather(tokens, xbuf, (tok_send, tok_recv, tokp_send, tokp_recv), project)
-    lax.fori_loop(1, nsp - s, send_shift, 0)
-
-    scale = lax.rsqrt(jnp.sum(squares[...], axis=1, keepdims=True) / model + epsilon)
-
-    def projected(i):
-        return (acc[:, i * width : (i + 1) * width] * scale).astype(BF16)
-
-    kvbuf[0, :, :width] = projected(3)
-    kvbuf[0, :, width:] = projected(4)
-
-    a = projected(0).astype(F32)
-    gate = projected(1).astype(F32)
-    gbuf[pl.ds(HALO, rows), :] = a / (1.0 + jnp.exp(-gate))
-
-    def kv_copy(d):
+            acc[rs, :] += part
+            squares[rs, :] += folded
+
+    def kv_copy(d, t):
+        rs = pl.ds(t * KEY_TILE, KEY_TILE)
         return pltpu.make_async_remote_copy(
-            src_ref=kvbuf.at[0],
-            dst_ref=kvbuf.at[d],
-            send_sem=kv_send.at[d],
-            recv_sem=kv_recv.at[d],
+            src_ref=kvbuf.at[0, rs],
+            dst_ref=kvbuf.at[d, rs],
+            send_sem=kv_send.at[d, t],
+            recv_sem=kv_recv.at[d, t],
             device_id={"sp": lax.rem(s + d, nsp)},
             device_id_type=MESH,
         )
@@ -261,23 +260,62 @@
         device_id_type=MESH,
     )
 
-    @pl.when(s + 1 < nsp)
-    def _():
-        halo.start()
-
-    def send_kv(d, carry):
-        kv_copy(d).start()
-        return carry
-
-    lax.fori_loop(1, nsp - s, send_kv, 0)
-
     lane = lax.broadcasted_iota(jnp.int32, (1, width), 1)
     head_lanes = [
         ((lane >= h * HEAD_DIM) & (lane < (h + 1) * HEAD_DIM)).astype(F32) for h in range(heads)
     ]
-    q = projected(2).astype(F32) * (HEAD_DIM**-0.5)
-    for h in range(heads):
-        qbuf[h] = (q * head_lanes[h]).astype(BF16)
+    tiles = rows // KEY_TILE
+    tok_sems = (tok_send, tok_recv, tokp_send, tokp_recv)
+    order = list(range(tiles - 1, -1, -1))
+
+    def own_rows(t):
+        return tokens.at[pl.ds(t * KEY_TILE, KEY_TILE)]
+
+    def token_view(t):
+        return lambda index: xbuf.at[index, pl.ds(t * KEY_TILE, KEY_TILE)]
+
+    for t in order:
+        start(own_rows(t), token_view(t), tok_sems, t * nfs)
+    lax.fori_loop(1, nsp - s, send_shift, 0)
+    for copy in locals_[:6]:
+        copy.wait()
+
+    for t in order:
+        row0 = t * KEY_TILE
+        rs = pl.ds(row0, KEY_TILE)
+        args = (own_rows(t), token_view(t), tok_sems, t * nfs)
+
+        def consume(index, row0=row0):
+            project(index, row0, False)
+
+        project(g, row0, True)
+        own_chip(*args, consume)
+        relay(*args, consume)
+        finish_relay(*args, consume)
+        scale = lax.rsqrt(jnp.sum(squares[rs, :], axis=1, keepdims=True) / model + epsilon)
+
+        def projected(i, rs=rs, scale=scale):
+            return (acc[rs, i * width : (i + 1) * width] * scale).astype(BF16)
+
+        kvbuf[0, rs, :width] = projected(3)
+        kvbuf[0, rs, width:] = projected(4)
+        a = projected(0).astype(F32)
+        gate = projected(1).astype(F32)
+        gbuf[pl.ds(HALO + row0, KEY_TILE), :] = a / (1.0 + jnp.exp(-gate))
+        if t == tiles - 1:
+
+            @pl.when(s + 1 < nsp)
+            def _():
+                halo.start()
+
+        def send_kv(d, carry, t=t):
+            kv_copy(d, t).start()
+            return carry
+
+        lax.fori_loop(1, nsp - s, send_kv, 0)
+        q = projected(2).astype(F32) * (HEAD_DIM**-0.5)
+        for h in range(heads):
+            qbuf[h, rs, :] = (q * head_lanes[h]).astype(BF16)
     obuf[...] = jnp.zeros_like(obuf)
     behind[...] = jnp.zeros_like(behind)
 
@@ -307,7 +345,6 @@
         obuf[rs, :] += jnp.dot(weights.astype(BF16), values, preferred_element_type=F32)
         behind[h, rs, :] = past + sums[:, :1]
 
-    tiles = rows // KEY_TILE
     for h in range(heads):
         for qt in range(tiles):
             for kt in range(qt, -1, -1):
@@ -368,33 +405,27 @@
     own_conv[...] = mixed
     cbuf[g] = mixed
 
-    def conv_copy(d, index):
-        return pltpu.make_async_remote_copy(
-            src_ref=own_conv,
-            dst_ref=cbuf.at[index],
-            send_sem=conv_send.at[d],
-            recv_sem=conv_recv.at[d],
-            device_id=in_group(lax.rem(g + d, group)),
-            device_id_type=MESH,
-        )
-
-    for d in range(1, group):
-        conv_copy(d, g).start()
+    conv_args = (own_conv, lambda index: cbuf.at[index], (conv_send, conv_recv, convp_send, convp_recv), 0)
+    start(*conv_args)
 
     def attend(d, carry):
         sh_copy(d).wait_recv()
-        kv_copy(d).wait_recv()
-        for h in range(heads):
-            for kt in range(tiles - 1, -1, -1):
+        for kt in order:
+            kv_copy(d, kt).wait_recv()
+            for h in range(heads):
                 tile(d, h, 0, rows, kt * KEY_TILE, False)
         return carry
 
-    lax.fori_loop(1, s + 1, attend, 0)
+    lax.fori_loop(1, s, attend, 0)
+    relay(*conv_args, None)
+    lax.fori_loop(jnp.maximum(s, 1), s + 1, attend, 0)
 
     attn = obuf[...].astype(BF16)
     own_attn[...] = attn
     abuf[g] = attn
 
+    attn_args = (own_attn, lambda index: abuf.at[index], (att_send, att_recv, attp_send, attp_recv), 0)
+    start(*attn_args)
     locals_[6].wait()
 
     def mix(buf, gain, base, index, first):
@@ -409,25 +440,24 @@
             acc[:, : out.shape[1]] += part
             squares[...] += v * v
 
-    def mix_conv():
-        mix(cbuf, conv_gain, 0, g, True)
-        for d in range(1, group):
-            origin = lax.rem(g + group - d, group)
-            conv_copy(d, origin).wait_recv()
-            mix(cbuf, conv_gain, 0, origin, False)
-        conv_scale = lax.rsqrt(
-            jnp.sum(squares[...], axis=1, keepdims=True) / channels + epsilon
-        )
-        out_width = out.shape[1]
-        acc[:, out_width : 2 * out_width] = acc[:, :out_width] * conv_scale
-
-    def mix_attn(index, first):
-        if first:
-            mix_conv()
-        mix(abuf, attn_gain, channels, index, first)
-
-    sent += gather(own_attn, abuf, (att_send, att_recv, attp_send, attp_recv), mix_attn)
+    def mix_conv(index):
+        mix(cbuf, conv_gain, 0, index, False)
+
+    def mix_attn(index):
+        mix(abuf, attn_gain, channels, index, False)
+
     out_width = out.shape[1]
+    mix(cbuf, conv_gain, 0, g, True)
+    own_chip(*conv_args, mix_conv)
+    for k in range(1, nfs):
+        mix_conv(chip_from(k) * ntp + c)
+    finish_relay(*conv_args, mix_conv)
+    conv_scale = lax.rsqrt(jnp.sum(squares[...], axis=1, keepdims=True) / channels + epsilon)
+    acc[:, out_width : 2 * out_width] = acc[:, :out_width] * conv_scale
+    mix(abuf, attn_gain, channels, g, True)
+    own_chip(*attn_args, mix_attn)
+    relay(*attn_args, mix_attn)
+    finish_relay(*attn_args, mix_attn)
     attn_scale = lax.rsqrt(jnp.sum(squares[...], axis=1, keepdims=True) / channels + epsilon)
     out[...] = (acc[:, out_width : 2 * out_width] + acc[:, :out_width] * attn_scale).astype(BF16)
 
@@ -435,7 +465,6 @@
         copy.wait_send()
     for d in range(1, group):
         stat_copy(d).wait_send()
-        conv_copy(d, g).wait_send()
 
     @pl.when(s + 1 < nsp)
     def _():
@@ -443,7 +472,8 @@
 
     def finish(d, carry):
         sh_copy(d).wait_send()
-        kv_copy(d).wait_send()
+        for t in range(tiles):
+            kv_copy(d, t).wait_send()
         return carry
 
     lax.fori_loop(1, nsp - s, finish, 0)
@@ -471,6 +501,7 @@
     width = conv_a_weight.shape[1]
     heads = break_shift.shape[0]
     out_width = out_weight.shape[1]
+    tiles = rows // KEY_TILE
     vm = pl.BlockSpec(memory_space=pltpu.VMEM)
     hbm = pl.BlockSpec(memory_space=pl.ANY)
     dma = pltpu.SemaphoreType.DMA
@@ -499,26 +530,28 @@
             pltpu.VMEM((rows, width), F32),
             pltpu.VMEM((heads, rows, LANES), F32),
             dma((7,)),
+            dma((tiles * nfs,)),
+            dma((tiles * nfs,)),
+            dma((ntp, tiles * nfs)),
+            dma((ntp, tiles * nfs)),
             dma((nfs,)),
             dma((nfs,)),
             dma((ntp, nfs)),
             dma((ntp, nfs)),
-            dma((nfs,)),
-            dma((nfs,)),
-            dma((ntp, nfs)),
-            dma((ntp, nfs)),
-            dma((nsp,)),
-            dma((nsp,)),
+            dma((nsp, tiles)),
+            dma((nsp, tiles)),
             dma((nsp,)),
             dma((nsp,)),
             dma((2,)),
             dma((group,)),
             dma((group,)),
-            dma((group,)),
-            dma((group,)),
+            dma((nfs,)),
+            dma((nfs,)),
+            dma((ntp, nfs)),
+            dma((ntp, nfs)),
         ],
         compiler_params=pltpu.CompilerParams(
-            collective_id=0, has_side_effects=True, vmem_limit_bytes=48 * 2**20
+            collective_id=0, has_side_effects=True, vmem_limit_bytes=67043328
         ),
         name="layer",
     )(

time: 71.8 us -> 56.3 us (0.78)
  local copies, waits for them, and re-layouts: 11.7 us -> 1.67 us
  Pallas kernels: 59.5 us -> 54.4 us
    unnamed x27 -> x1, local copies, waits for them, and re-layouts: 11.7 us -> 1.67 us
    pallas_call x1, Pallas kernels: 59.5 us -> 54.4 us  [per_device(): pl.pallas_call(functools.partial(layer_kernel, nsp, nfs, ntp), out_shape=...]
where the time goes in v2:
time: 56.3 us; the launch traced here: 56.1 us
  Pallas kernels  54.4 us (97%)
  local copies, waits for them, and re-layouts  1.67 us (3%)
    pallas_call x1, Pallas kernels, per_device(): pl.pallas_call(functools.partial(layer_kernel, nsp, nfs, ntp), out_shape=...  54.4 us
    unnamed x1, local copies, waits for them, and re-layouts  1.67 us

profile of v2, /device:TPU:25, one launch (start us, length us, event | category | flops | bytes accessed | tf_op | source)
XLA Modules:
  0.0 56.1 jit_solution(1924505268705711144)
XLA Ops:
  0.0 54.4 %layer.1 = bf16[512,256]{1,0:T(8,128)(2,1)} custom-call(bf16[512,256]{1,0:T(8,128)(2,1)} %tokens.1, bf16[2048,128]{1,0:T(8,128)(2,1)} %w_a.1, bf16[2048,128]{1,0:T(8,128)(2,1)} %w_gate.1, bf16[2048,128]{1,0:T(8,128)(2,1)} %w_q.1, bf16[2048,128]{1,0:T(8,128)(2,1)} %w_k.1, bf16[2048,128]{1,0:T(8,128)(2,1)} %w_v.1, bf16[2048,256]{1,0:T(8,128)(2,1)} %w_out.1, ...), custom_call_target="tpu_custom_call" | custom-call | tf_op jit(solution)/shard_map/layer/pallas_call | solution.py:508
  54.4 1.7 %copy.15 = bf16[512,256]{1,0:T(8,128)(2,1)} copy(bf16[512,256]{1,0:T(8,128)(2,1)} %layer.1) | data formatting | bytes 524288

commit v3 on v2

--- a/solution.py
+++ b/solution.py
@@ -418,48 +418,84 @@
 
     lax.fori_loop(1, s, attend, 0)
     relay(*conv_args, None)
-    lax.fori_loop(jnp.maximum(s, 1), s + 1, attend, 0)
-
-    attn = obuf[...].astype(BF16)
-    own_attn[...] = attn
-    abuf[g] = attn
-
-    attn_args = (own_attn, lambda index: abuf.at[index], (att_send, att_recv, attp_send, attp_recv), 0)
-    start(*attn_args)
+    att_sems = (att_send, att_recv, attp_send, attp_recv)
+
+    def attn_rows(t):
+        return own_attn.at[pl.ds(t * KEY_TILE, KEY_TILE)]
+
+    def attn_view(t):
+        return lambda index: abuf.at[index, pl.ds(t * KEY_TILE, KEY_TILE)]
+
+    for qt in order:
+
+        def attend_part(d, carry, qt=qt):
+            if qt == order[0]:
+                sh_copy(d).wait_recv()
+            for kt in order:
+                if qt == order[0]:
+                    kv_copy(d, kt).wait_recv()
+                for h in range(heads):
+                    tile(d, h, qt * KEY_TILE, KEY_TILE, kt * KEY_TILE, False)
+            return carry
+
+        lax.fori_loop(jnp.maximum(s, 1), s + 1, attend_part, 0)
+        rs = pl.ds(qt * KEY_TILE, KEY_TILE)
+        attn = obuf[rs, :].astype(BF16)
+        own_attn[rs, :] = attn
+        abuf[g, rs, :] = attn
+        start(attn_rows(qt), attn_view(qt), att_sems, qt * nfs)
     locals_[6].wait()
 
-    def mix(buf, gain, base, index, first):
-        v = buf[index].astype(F32)
-        scaled = (v * gain[pl.ds(index, 1), :]).astype(BF16)
-        w = wout[pl.ds(pl.multiple_of(base + index * width, width), width), :]
+    def mix_attn(index, row0, first):
+        rs = pl.ds(row0, KEY_TILE)
+        v = abuf[index, rs, :].astype(F32)
+        scaled = (v * attn_gain[pl.ds(index, 1), :]).astype(BF16)
+        w = wout[pl.ds(pl.multiple_of(channels + index * width, width), width), :]
         part = jnp.dot(scaled, w, preferred_element_type=F32)
         if first:
-            acc[:, : out.shape[1]] = part
-            squares[...] = v * v
+            acc[rs, :out_width] = part
+            squares[rs, :] = v * v
         else:
-            acc[:, : out.shape[1]] += part
-            squares[...] += v * v
-
-    def mix_conv(index):
-        mix(cbuf, conv_gain, 0, index, False)
-
-    def mix_attn(index):
-        mix(abuf, attn_gain, channels, index, False)
+            acc[rs, :out_width] += part
+            squares[rs, :] += v * v
+
+    def nothing(index):
+        return None
 
     out_width = out.shape[1]
-    mix(cbuf, conv_gain, 0, g, True)
-    own_chip(*conv_args, mix_conv)
-    for k in range(1, nfs):
-        mix_conv(chip_from(k) * ntp + c)
-    finish_relay(*conv_args, mix_conv)
-    conv_scale = lax.rsqrt(jnp.sum(squares[...], axis=1, keepdims=True) / channels + epsilon)
-    acc[:, out_width : 2 * out_width] = acc[:, :out_width] * conv_scale
-    mix(abuf, attn_gain, channels, g, True)
-    own_chip(*attn_args, mix_attn)
-    relay(*attn_args, mix_attn)
-    finish_relay(*attn_args, mix_attn)
-    attn_scale = lax.rsqrt(jnp.sum(squares[...], axis=1, keepdims=True) / channels + epsilon)
-    out[...] = (acc[:, out_width : 2 * out_width] + acc[:, :out_width] * attn_scale).astype(BF16)
+    own_chip(*conv_args, nothing)
+    finish_relay(*conv_args, nothing)
+    for t in order:
+        rs = pl.ds(t * KEY_TILE, KEY_TILE)
+        pieces = []
+        folded = jnp.zeros((KEY_TILE, width), F32)
+        for index in range(group):
+            v = cbuf[index, rs, :].astype(F32)
+            folded = folded + v * v
+            pieces.append((v * conv_gain[index : index + 1, :]).astype(BF16))
+        product = jnp.dot(
+            jnp.concatenate(pieces, axis=1), wout[:channels, :], preferred_element_type=F32
+        )
+        conv_scale = lax.rsqrt(jnp.sum(folded, axis=1, keepdims=True) / channels + epsilon)
+        acc[rs, out_width : 2 * out_width] = product * conv_scale
+    for t in order:
+        row0 = t * KEY_TILE
+        rs = pl.ds(row0, KEY_TILE)
+        args = (attn_rows(t), attn_view(t), att_sems, t * nfs)
+
+        def consume_attn(index, row0=row0):
+            mix_attn(index, row0, False)
+
+        mix_attn(g, row0, True)
+        own_chip(*args, consume_attn)
+        relay(*args, consume_attn)
+        finish_relay(*args, consume_attn)
+        attn_scale = lax.rsqrt(
+            jnp.sum(squares[rs, :], axis=1, keepdims=True) / channels + epsilon
+        )
+        out[rs, :] = (
+            acc[rs, out_width : 2 * out_width] + acc[rs, :out_width] * attn_scale
+        ).astype(BF16)
 
     for copy in sent:
         copy.wait_send()
@@ -534,10 +570,10 @@
             dma((tiles * nfs,)),
             dma((ntp, tiles * nfs)),
             dma((ntp, tiles * nfs)),
-            dma((nfs,)),
-            dma((nfs,)),
-            dma((ntp, nfs)),
-            dma((ntp, nfs)),
+            dma((tiles * nfs,)),
+            dma((tiles * nfs,)),
+            dma((ntp, tiles * nfs)),
+            dma((ntp, tiles * nfs)),
             dma((nsp, tiles)),
             dma((nsp, tiles)),
             dma((nsp,)),

time: 56.3 us -> 55.5 us (0.986)
  Pallas kernels: 54.4 us -> 53.7 us
    pallas_call x1, Pallas kernels: 54.4 us -> 53.7 us  [per_device(): pl.pallas_call(functools.partial(layer_kernel, nsp, nfs, ntp), out_shape=...]
where the time goes in v3:
time: 55.5 us; the launch traced here: 55.3 us
  Pallas kernels  53.7 us (97%)
  local copies, waits for them, and re-layouts  1.67 us (3%)
    pallas_call x1, Pallas kernels, per_device(): pl.pallas_call(functools.partial(layer_kernel, nsp, nfs, ntp), out_shape=...  53.7 us
    unnamed x1, local copies, waits for them, and re-layouts  1.67 us

profile of v3, /device:TPU:25, one launch (start us, length us, event | category | flops | bytes accessed | tf_op | source)
XLA Modules:
  0.0 55.3 jit_solution(13277132836064466423)
XLA Ops:
  0.0 53.7 %layer.1 = bf16[512,256]{1,0:T(8,128)(2,1)} custom-call(bf16[512,256]{1,0:T(8,128)(2,1)} %tokens.1, bf16[2048,128]{1,0:T(8,128)(2,1)} %w_a.1, bf16[2048,128]{1,0:T(8,128)(2,1)} %w_gate.1, bf16[2048,128]{1,0:T(8,128)(2,1)} %w_q.1, bf16[2048,128]{1,0:T(8,128)(2,1)} %w_k.1, bf16[2048,128]{1,0:T(8,128)(2,1)} %w_v.1, bf16[2048,256]{1,0:T(8,128)(2,1)} %w_out.1, ...), custom_call_target="tpu_custom_call" | custom-call | tf_op jit(solution)/shard_map/layer/pallas_call | solution.py:544
  53.7 1.7 %copy.15 = bf16[512,256]{1,0:T(8,128)(2,1)} copy(bf16[512,256]{1,0:T(8,128)(2,1)} %layer.1) | data formatting | bytes 524288
